TPU v7x, 32 devices: a whole 2x2x4 slice. The times are simulated.
32 devices in a mesh: fs: 8 (over z, x), tp: 4 (over y, core).
Axes of the slice: x: 2, y: 2, z: 4, core: 2. Of those that a mesh axis runs over, the one named last changes fastest.
Arguments:
- mixer_input: bfloat16 [8192, 4096], P('fs'), may hold values from -6 to 6
- cell_output: bfloat16 [8192, 2048], P('fs'), may hold values from -6 to 6
- query_grad: bfloat16 [8192, 2048], P('fs', 'tp'), may hold values from -4 to 4
- value_grad: bfloat16 [8192, 2048], P('fs', 'tp'), may hold values from -4 to 4
- output_grad: bfloat16 [8192, 4096], P('fs', 'tp'), may hold values from -4 to 4
- query_weight: float32 [4096, 2048], P('fs', 'tp'), may hold values from -6 to 6
- value_weight: float32 [4096, 2048], P('fs', 'tp'), may hold values from -6 to 6
- output_weight: float32 [2048, 4096], P('fs', 'tp'), may hold values from -6 to 6
- query_basis: bfloat16 [4096, 128], P('fs'), may hold values from -0.09375 to 0.09375
- value_basis: bfloat16 [4096, 128], P('fs'), may hold values from -0.09375 to 0.09375
- output_basis: bfloat16 [2048, 128], P('fs'), may hold values from -0.125 to 0.125
- query_mean: float32 [128, 2048], P(None, 'tp'), may hold values from -6 to 6
- value_mean: float32 [128, 2048], P(None, 'tp'), may hold values from -6 to 6
- output_mean: float32 [128, 4096], P(None, 'tp'), may hold values from -6 to 6
- query_square: float32 [128, 2048], P(None, 'tp'), may hold values from 0.25 to 4
- value_square: float32 [128, 2048], P(None, 'tp'), may hold values from 0.25 to 4
- output_square: float32 [128, 4096], P(None, 'tp'), may hold values from 0.25 to 4
Outputs:
- query_step: float32 [4096, 2048], P('fs', 'tp')
- value_step: float32 [4096, 2048], P('fs', 'tp')
- output_step: float32 [2048, 4096], P('fs', 'tp')
- query_copy: bfloat16 [4096, 2048], P(None, 'tp')
- value_copy: bfloat16 [4096, 2048], P(None, 'tp')
- output_copy: bfloat16 [2048, 4096], P(None, 'tp')
- query_first: float32 [128, 2048], P(None, 'tp')
- value_first: float32 [128, 2048], P(None, 'tp')
- output_first: float32 [128, 4096], P(None, 'tp')
- query_second: float32 [128, 2048], P(None, 'tp')
- value_second: float32 [128, 2048], P(None, 'tp')
- output_second: float32 [128, 4096], P(None, 'tp')
All inputs are finite; a program needn't handle non-finite values.
Results may differ from a plain program's by a relative error of at most 0.013.
Values may be sent and summed in bfloat16 or wider, within the bound.
A program may use at most 128 MiB of HBM per device.

v0:
```python
import functools

import jax
import jax.numpy as jnp
from jax import lax
from jax.experimental import pallas as pl
from jax.experimental.pallas import tpu as pltpu
from jax.sharding import PartitionSpec as P

MODEL = 4096
CELL = 2048


beta_first = 0.8
beta_second = 0.9
floor_mean = 0.005
learn_rate = 0.05

MESH = pl.DeviceIdType.MESH


def matmul(left, right):
    return jnp.dot(left, right, preferred_element_type=jnp.float32)


def split(value):
    high = lax.reduce_precision(value, 8, 7)
    return high.astype(jnp.bfloat16), (value - high).astype(jnp.bfloat16)


def moments(projected, mean_old, square_old):
    moment_one = beta_first * mean_old + (1.0 - beta_first) * projected
    moment_two = beta_second * square_old + (1.0 - beta_second) * projected * projected
    return (moment_one, moment_two, moment_one / jnp.sqrt(moment_two))


def twice(basis):
    return jnp.concatenate([basis, basis], axis=1)


class Gather:
    def __init__(self, number, own, whole, me, count, parity, send_sem, recv_sem):
        self.number, self.own, self.whole, self.me = number, own, whole, me
        self.count, self.parity = count, parity
        self.send_sem, self.recv_sem = send_sem, recv_sem
        self.rows = whole.shape[0] // count
        self.sent = []
        self.relayed = count == 8
        place, side = me // 2, lax.rem(me, 2)
        self.cross = place * 2 + (1 - side)
        self.up = lax.rem(place + 1, 4) * 2 + side
        self.down = lax.rem(place + 3, 4) * 2 + side
        up_cross = lax.rem(place + 1, 4) * 2 + (1 - side)
        down_cross = lax.rem(place + 3, 4) * 2 + (1 - side)
        far = lax.rem(place + 2, 4) * 2 + side
        far_cross = lax.rem(place + 2, 4) * 2 + (1 - side)
        if self.relayed:
            self.origins = [
                self.cross, self.down, self.up, down_cross, up_cross, far, far_cross
            ]
        else:
            self.origins = [lax.rem(me + count - k, count) for k in range(1, count)]

    def slot(self, origin):
        return self.whole.at[pl.ds(pl.multiple_of(origin * self.rows, self.rows), self.rows), :]

    def copy(self, role, source, origin, target):
        return pltpu.make_async_remote_copy(
            src_ref=source,
            dst_ref=self.slot(origin),
            send_sem=self.send_sem.at[self.number, role],
            recv_sem=self.recv_sem.at[self.number, role],
            device_id={"fs": target},
            device_id_type=MESH,
        )

    def send(self, role, origin, target, source=None):
        copy = self.copy(role, self.slot(origin) if source is None else source, origin, target)
        copy.start()
        self.sent.append(copy)

    def arrive(self, role):
        origin = self.origins[role]
        self.copy(role, self.slot(origin), origin, self.cross).wait_recv()

    def start(self):
        if self.relayed:
            for role, target in enumerate((self.cross, self.up, self.down)):
                self.send(role, self.me, target, self.own)
        else:
            for k in range(1, self.count):
                self.send(k - 1, self.me, lax.rem(self.me + k, self.count), self.own)

    def middle(self):
        if self.relayed:
            self.arrive(0)
            self.send(3, self.origins[0], self.up)
            self.send(4, self.origins[0], self.down)
            self.arrive(1)
            if self.parity:
                self.send(5, self.origins[1], self.up)
            self.arrive(2)
            if not self.parity:
                self.send(5, self.origins[2], self.down)

    def late(self):
        if self.relayed:
            self.arrive(5)
            self.send(6, self.origins[5], self.cross)

    def finish(self):
        for role in (3, 4, 6) if self.relayed else range(self.count - 1):
            self.arrive(role)

    def drain(self):
        for copy in self.sent:
            copy.wait_send()


def kernel(
    fs,
    tp,
    mixer_hbm,
    cell_hbm,
    qg_hbm,
    vg_hbm,
    og_hbm,
    pair_hbm,
    ob_hbm,
    qw_hbm,
    vw_hbm,
    ow_hbm,
    qm,
    vm,
    om,
    qs,
    vs,
    os,
    qw_all,
    vw_all,
    ow_all,
    pair_all,
    ob_all,
    proj,
    squares,
    mixer,
    cell,
    qg,
    vg,
    og,
    qw,
    vw,
    ow,
    part,
    parts,
    square_own,
    square_in,
    send_sem,
    recv_sem,
    sum_send,
    sum_recv,
    all_send,
    all_recv,
    tp_send,
    tp_recv,
    local_sem,
):
    me, column = lax.axis_index("fs"), lax.axis_index("tp")
    rank, width = qm.shape
    gathers = [
        Gather(i, own, whole, me, fs, parity, send_sem, recv_sem)
        for i, (own, whole, parity) in enumerate(
            ((None, pair_all, 0), (None, ob_all, 1), (qw, qw_all, 0), (vw, vw_all, 1), (ow, ow_all, 0))
        )
    ]
    for gather in gathers[:2]:
        gather.own = gather.slot(me)
    loads = [
        pltpu.make_async_copy(source, target, local_sem.at[i])
        for i, (source, target) in enumerate(
            (
                (pair_hbm, gathers[0].own),
                (ob_hbm, gathers[1].own),
                (qw_hbm, qw),
                (vw_hbm, vw),
                (ow_hbm, ow),
                (cell_hbm, cell),
                (og_hbm, og),
                (mixer_hbm, mixer),
                (qg_hbm, qg),
                (vg_hbm, vg),
            )
        )
    ]
    for load in loads:
        load.start()

    barrier = pltpu.get_barrier_semaphore()
    for k in range(1, fs):
        pl.semaphore_signal(
            barrier, inc=1, device_id={"fs": lax.rem(me + k, fs)}, device_id_type=MESH
        )
    for k in range(1, tp):
        pl.semaphore_signal(
            barrier, inc=1, device_id={"tp": lax.rem(column + k, tp)}, device_id_type=MESH
        )
    pl.semaphore_wait(barrier, fs + tp - 2)

    pair_g, ob_g, qw_g, vw_g, ow_g = gathers
    loads[0].wait()
    pair_g.start()
    loads[1].wait()
    ob_g.start()
    loads[2].wait()
    qw_g.start()
    pair_g.middle()
    ob_g.middle()
    pair_g.late()
    ob_g.late()
    loads[3].wait()
    vw_g.start()
    loads[4].wait()
    ow_g.start()
    keeps = [
        pltpu.make_async_copy(gather.own, gather.slot(me), local_sem.at[10 + i])
        for i, gather in enumerate(gathers[2:])
    ]
    for keep in keeps:
        keep.start()
    qw_g.middle()
    for load in loads[5:]:
        load.wait()
    part[...] = jnp.zeros_like(part)
    pair_g.finish()
    ob_g.finish()

    tile = 256

    def project(rows, grad):
        turned = jnp.transpose(rows)
        high = turned.astype(jnp.bfloat16)
        low = (turned - high.astype(jnp.float32)).astype(jnp.bfloat16)
        both = matmul(jnp.concatenate([high, low], axis=0), grad)
        return both[:rank] + both[rank:]

    def step(t, carry):
        at = pl.ds(pl.multiple_of(t * tile, tile), tile)
        rows = matmul(mixer[at, :], pair_all[...])
        part[:, :width] += project(rows[:, :rank], qg[at, :])
        part[:, width : 2 * width] += project(rows[:, rank:], vg[at, :])
        part[:, 2 * width :] += project(matmul(cell[at, :], ob_all[...]), og[at, :])
        return carry

    lax.fori_loop(0, mixer.shape[0] // tile, step, 0)

    share = rank // fs

    def strip(index):
        return pl.ds(pl.multiple_of(index * share, share), share)

    sums = []
    for k in range(1, fs):
        target = lax.rem(me + k, fs)
        copy = pltpu.make_async_remote_copy(
            src_ref=part.at[strip(target), :],
            dst_ref=parts.at[k - 1],
            send_sem=sum_send.at[k - 1],
            recv_sem=sum_recv.at[k - 1],
            device_id={"fs": target},
            device_id_type=MESH,
        )
        copy.start()
        sums.append(copy)
    vw_g.middle()
    qw_g.late()

    def gram(whole, block):
        def add(i, total):
            piece = whole[pl.ds(pl.multiple_of(i * block, block), block), :]
            turned = jnp.transpose(piece.astype(jnp.float32)).astype(jnp.bfloat16)
            return total + matmul(turned, piece)

        size = whole.shape[1]
        return lax.fori_loop(
            0, whole.shape[0] // block, add, jnp.zeros((size, size), jnp.float32)
        )

    for copy in sums:
        copy.wait_recv()
    total = part[strip(me), :]
    for k in range(1, fs):
        total = total + parts[k - 1]
    proj[strip(me), :] = total
    gram_pair = gram(pair_all, 256)
    gram_output = gram(ob_all, 256)
    alls = []
    for k in range(1, fs):
        copy = pltpu.make_async_remote_copy(
            src_ref=proj.at[strip(me), :],
            dst_ref=proj.at[strip(me), :],
            send_sem=all_send.at[k - 1],
            recv_sem=all_recv.at[k - 1],
            device_id={"fs": lax.rem(me + k, fs)},
            device_id_type=MESH,
        )
        copy.start()
        alls.append(copy)
    ow_g.middle()
    vw_g.late()
    for k in range(1, fs):
        origin = lax.rem(me + fs - k, fs)
        pltpu.make_async_remote_copy(
            src_ref=proj.at[strip(origin), :],
            dst_ref=proj.at[strip(origin), :],
            send_sem=all_send.at[k - 1],
            recv_sem=all_recv.at[k - 1],
            device_id={"fs": lax.rem(me + k, fs)},
            device_id_type=MESH,
        ).wait_recv()

    def norm(basis_gram, projected, mean, square):
        direction = moments(projected, mean[...], square[...])[2]
        turned = jnp.dot(
            basis_gram,
            direction,
            precision=lax.Precision.HIGHEST,
            preferred_element_type=jnp.float32,
        )
        lanes = jnp.sum(direction * turned, axis=0, keepdims=True)
        return jnp.sum(lanes, axis=1, keepdims=True)

    partial = (
        norm(gram_pair[:rank, :rank], proj[:, :width], qm, qs)
        + norm(gram_pair[rank:, rank:], proj[:, width : 2 * width], vm, vs)
        + norm(gram_output, proj[:, 2 * width :], om, os)
    )
    square_own[...] = jnp.broadcast_to(partial, square_own.shape)
    ow_g.late()
    shares = []
    for k in range(1, tp):
        copy = pltpu.make_async_remote_copy(
            src_ref=square_own,
            dst_ref=square_in.at[k - 1],
            send_sem=tp_send.at[k - 1],
            recv_sem=tp_recv.at[k - 1],
            device_id={"tp": lax.rem(column + k, tp)},
            device_id_type=MESH,
        )
        copy.start()
        shares.append(copy)
    for copy in shares:
        copy.wait_recv()
    whole_squares = square_own[...]
    for k in range(1, tp):
        whole_squares = whole_squares + square_in[k - 1]
    squares[...] = whole_squares
    for gather in gathers[2:]:
        gather.finish()
    for copy in sums + alls + shares:
        copy.wait_send()
    for gather in gathers:
        gather.drain()
    for keep in keeps:
        keep.wait()


def exchange(fs, tp, mixer, cell, grads, pair, output_basis, weights, means, olds):
    share = pair.shape[1] // 2 // fs
    total = sum(grad.shape[1] for grad in grads)
    rank = means[0].shape[0]
    bf16, f32 = jnp.bfloat16, jnp.float32
    places = max(fs - 1, 7)
    hbm, vmem = pl.BlockSpec(memory_space=pl.ANY), pl.BlockSpec(memory_space=pltpu.VMEM)
    dma = pltpu.SemaphoreType.DMA

    def whole(array):
        return jax.ShapeDtypeStruct((array.shape[0] * fs, array.shape[1]), bf16)

    return pl.pallas_call(
        functools.partial(kernel, fs, tp),
        out_shape=(
            *(whole(weight) for weight in weights),
            whole(pair),
            whole(output_basis),
            jax.ShapeDtypeStruct((rank, total), f32),
            jax.ShapeDtypeStruct((8, 128), f32),
        ),
        in_specs=[hbm] * 10 + [vmem] * 6,
        out_specs=(hbm,) * 3 + (vmem,) * 4,
        scratch_shapes=[
            *(pltpu.VMEM(array.shape, bf16) for array in (mixer, cell, *grads, *weights)),
            pltpu.VMEM((rank, total), f32),
            pltpu.VMEM((fs - 1, share, total), f32),
            pltpu.VMEM((8, 128), f32),
            pltpu.VMEM((tp - 1, 8, 128), f32),
            dma((5, places)),
            dma((5, places)),
            dma((fs - 1,)),
            dma((fs - 1,)),
            dma((fs - 1,)),
            dma((fs - 1,)),
            dma((tp - 1,)),
            dma((tp - 1,)),
            dma((13,)),
        ],
        compiler_params=pltpu.CompilerParams(
            collective_id=0, has_side_effects=True, vmem_limit_bytes=50 * 1024 * 1024
        ),
    )(mixer, cell, *grads, pair, output_basis, *weights, *means, *olds)


def body(fs, tp):
    def local(
        mixer_input,
        cell_output,
        query_grad,
        value_grad,
        output_grad,
        query_weight,
        value_weight,
        output_weight,
        query_basis,
        value_basis,
        output_basis,
        query_mean,
        value_mean,
        output_mean,
        query_square,
        value_square,
        output_square,
    ):
        rank = query_basis.shape[1]
        means = (query_mean, value_mean, output_mean)
        olds = (query_square, value_square, output_square)
        *weights, whole_pair, whole_output, projected, squares = exchange(
            fs,
            tp,
            mixer_input,
            cell_output,
            (query_grad, value_grad, output_grad),
            jnp.concatenate([query_basis, value_basis], axis=1),
            output_basis,
            [w.astype(jnp.bfloat16) for w in (query_weight, value_weight, output_weight)],
            means,
            olds,
        )
        width = query_grad.shape[1]
        proj = (
            projected[:, :width],
            projected[:, width : 2 * width],
            projected[:, 2 * width :],
        )
        firsts, seconds, dirs = zip(*(moments(*each) for each in zip(proj, means, olds)))
        bases = (whole_pair[:, :rank], whole_pair[:, rank:], whole_output)
        factor = 1.0 / jnp.sqrt(squares[0, 0] / (3.0 * MODEL * CELL) + floor_mean)
        pairs = [jnp.concatenate(split(d), axis=0) for d in dirs]
        steps = [
            -factor * matmul(twice(b), d)
            for b, d in zip((query_basis, value_basis, output_basis), pairs)
        ]
        copies = [
            (w.astype(jnp.float32) + (-learn_rate * factor) * matmul(twice(b), d)).astype(
                jnp.bfloat16
            )
            for w, b, d in zip(weights, bases, pairs)
        ]
        return (*steps, *copies, *firsts, *seconds)

    return local


def solution(mesh):
    rows, split_both, columns = P("fs", None), P("fs", "tp"), P(None, "tp")
    in_specs = (rows,) * 2 + (split_both,) * 6 + (rows,) * 3 + (columns,) * 6
    out_specs = (split_both,) * 3 + (columns,) * 9
    return jax.shard_map(
        body(mesh.shape["fs"], mesh.shape["tp"]),
        mesh=mesh,
        in_specs=in_specs,
        out_specs=out_specs,
        check_vma=False,
    )
```

profile of v0, /device:TPU:12, one launch (start us, length us, event | category | flops | bytes accessed | tf_op | source)
XLA Modules:
  0.0 293.0 jit_solution(18068599485966030555)
XLA Ops:
  0.7 1.4 convert_element_type.45.qw_hbm
  2.2 1.3 convert_element_type.46.vw_hbm
  3.4 1.3 convert_element_type.47.ow_hbm
  4.9 270.7 %shard_map.256 = (bf16[4096,512]{1,0:T(8,128)(2,1)}, bf16[4096,512]{1,0:T(8,128)(2,1)}, bf16[2048,1024]{1,0:T(8,128)(2,1)}, bf16[4096,256]{1,0:T(8,128)(2,1)}, b...) custom-call(bf16[1024,4096]{1,0:T(8,128)(2,1)} %mixer_hbm.1, bf16[1024,2048]{1,0:T(8,128)(2,1)} %cell_hbm.1, ...), custom_call_target="tpu_custom_call" | custom-call | tf_op jit(solution)/shard_map/pallas_call | solution.py:379
  275.6 1.4 reduce-precision_convert_fusion.1
  277.0 0.0 copy-start.11
  277.0 0.0 copy-start.12
  277.0 0.0 copy-start.13
  277.0 0.0 copy-start.14
  277.0 0.1 fusion.11
  277.1 0.5 slice.18
  278.6 0.1 fusion.29
  278.8 0.1 copy-done.19
  278.9 3.3 %add_convert_fusion.1 = bf16[4096,512]{1,0:T(8,128)(2,1)} fusion(bf16[4096,512]{1,0:T(8,128)(2,1)S(1)} %copy-done.19, f32[]{:T(128)} %bitcast.1, bf16[4096,128]{1,0:T(8,128)(2,1)S(1)} %get-tuple-element.35, bf16[128,512]{1,0:T(8,128)(2,1)S(1)} %get-tuple-element.41, bf16[128,512]{1,0:T(8,128)(2,1)S(1)} %get-tuple-element.29), kind=kOutput, calls=%fused_computation.1 | convolution fusion | flops 1086849024 | bytes 9699332 | tf_op jit(solution)/shard_map/dot_general | solution.py:23
  282.2 0.0 copy-start.7
  282.2 3.3 %add_convert_fusion.2 = bf16[4096,512]{1,0:T(8,128)(2,1)} fusion(bf16[4096,512]{1,0:T(8,128)(2,1)S(1)} %copy-done.18, f32[]{:T(128)} %bitcast.1, bf16[4096,128]{1,0:T(8,128)(2,1)S(1)} %get-tuple-element.36, bf16[128,512]{1,0:T(8,128)(2,1)S(1)} %get-tuple-element.40, bf16[128,512]{1,0:T(8,128)(2,1)S(1)} %get-tuple-element.37), kind=kOutput, calls=%fused_computation.2 | convolution fusion | flops 1086849024 | bytes 9699332 | tf_op jit(solution)/shard_map/dot_general | solution.py:23
  285.5 1.3 convolution_multiply_fusion.1
  286.8 1.3 convolution_multiply_fusion.2
  288.0 0.3 reduce-precision_convert_fusion
  288.3 0.0 copy-start.8
  288.3 0.0 copy-start.9
  288.3 0.1 fusion.9
  288.4 3.3 %add_convert_fusion = bf16[2048,1024]{1,0:T(8,128)(2,1)} fusion(bf16[2048,1024]{1,0:T(8,128)(2,1)S(1)} %copy-done.17, f32[]{:T(128)} %bitcast.1, bf16[2048,128]{1,0:T(8,128)(2,1)S(1)} %get-tuple-element.25, bf16[128,1024]{1,0:T(8,128)(2,1)S(1)} %fusion.9, bf16[128,1024]{1,0:T(8,128)(2,1)S(1)} %get-tuple-element.26), kind=kOutput, calls=%fused_computation | convolution fusion | flops 1085276160 | bytes 9437188 | tf_op jit(solution)/shard_map/dot_general | solution.py:23
  291.7 1.3 convolution_multiply_fusion
  (33 shorter events, 0.1 us)
Async XLA Ops:
  0.6 4.1 %copy-start.16 = (bf16[512,128]{1,0:T(8,128)(2,1)S(1)}, bf16[512,128]{1,0:T(8,128)(2,1)}, u32[]{:S(2)}) copy-start(bf16[512,128]{1,0:T(8,128)(2,1)} %param.25) | copy-start | bytes 393220
  0.7 4.1 %copy-start.15 = (bf16[512,128]{1,0:T(8,128)(2,1)S(1)}, bf16[512,128]{1,0:T(8,128)(2,1)}, u32[]{:S(2)}) copy-start(bf16[512,128]{1,0:T(8,128)(2,1)} %param.26) | copy-start | bytes 393220
  0.7 4.1 %copy-start.5 = (bf16[256,128]{1,0:T(8,128)(2,1)S(1)}, bf16[256,128]{1,0:T(8,128)(2,1)}, u32[]{:S(2)}) copy-start(bf16[256,128]{1,0:T(8,128)(2,1)} %ob_hbm.1) | copy-start | bytes 196612
  0.7 4.1 %copy-start.1 = (f32[128,512]{1,0:T(8,128)S(1)}, f32[128,512]{1,0:T(8,128)}, u32[]{:S(2)}) copy-start(f32[128,512]{1,0:T(8,128)} %qm.1) | copy-start | bytes 786436
  0.7 4.1 %copy-start.2 = (f32[128,512]{1,0:T(8,128)S(1)}, f32[128,512]{1,0:T(8,128)}, u32[]{:S(2)}) copy-start(f32[128,512]{1,0:T(8,128)} %vm.1) | copy-start | bytes 786436
  0.7 4.1 %copy-start = (f32[128,1024]{1,0:T(8,128)S(1)}, f32[128,1024]{1,0:T(8,128)}, u32[]{:S(2)}) copy-start(f32[128,1024]{1,0:T(8,128)} %om.1) | copy-start | bytes 1572868
  0.7 4.1 %copy-start.3 = (f32[128,512]{1,0:T(8,128)S(1)}, f32[128,512]{1,0:T(8,128)}, u32[]{:S(2)}) copy-start(f32[128,512]{1,0:T(8,128)} %qs.1) | copy-start | bytes 786436
  0.7 4.1 %copy-start.4 = (f32[128,512]{1,0:T(8,128)S(1)}, f32[128,512]{1,0:T(8,128)}, u32[]{:S(2)}) copy-start(f32[128,512]{1,0:T(8,128)} %vs.1) | copy-start | bytes 786436
  275.5 3.1 %copy-start.6 = (bf16[4096,256]{1,0:T(8,128)(2,1)S(1)}, bf16[4096,256]{1,0:T(8,128)(2,1)}, u32[]{:S(2)}) copy-start(bf16[4096,256]{1,0:T(8,128)(2,1)} %get-tuple-element.22) | copy-start | bytes 6291460
  275.6 3.4 %copy-start.19 = (bf16[4096,512]{1,0:T(8,128)(2,1)S(1)}, bf16[4096,512]{1,0:T(8,128)(2,1)}, u32[]{:S(2)}) copy-start(bf16[4096,512]{1,0:T(8,128)(2,1)} %get-tuple-element.23) | copy-start | bytes 12582916
  277.0 5.2 %copy-start.11 = (f32[128,512]{1,0:T(8,128)}, f32[128,512]{1,0:T(8,128)S(1)}, u32[]{:S(2)}) copy-start(f32[128,512]{1,0:T(8,128)S(1)} %get-tuple-element.30) | copy-start | bytes 786436
  277.0 5.2 %copy-start.12 = (f32[128,512]{1,0:T(8,128)}, f32[128,512]{1,0:T(8,128)S(1)}, u32[]{:S(2)}) copy-start(f32[128,512]{1,0:T(8,128)S(1)} %get-tuple-element.31) | copy-start | bytes 786436
  277.0 5.2 %copy-start.13 = (f32[128,512]{1,0:T(8,128)}, f32[128,512]{1,0:T(8,128)S(1)}, u32[]{:S(2)}) copy-start(f32[128,512]{1,0:T(8,128)S(1)} %get-tuple-element.38) | copy-start | bytes 786436
  277.0 5.2 %copy-start.14 = (f32[128,512]{1,0:T(8,128)}, f32[128,512]{1,0:T(8,128)S(1)}, u32[]{:S(2)}) copy-start(f32[128,512]{1,0:T(8,128)S(1)} %get-tuple-element.39) | copy-start | bytes 786436
  278.9 3.3 %copy-start.18 = (bf16[4096,512]{1,0:T(8,128)(2,1)S(1)}, bf16[4096,512]{1,0:T(8,128)(2,1)}, u32[]{:S(2)}) copy-start(bf16[4096,512]{1,0:T(8,128)(2,1)} %get-tuple-element.21) | copy-start | bytes 12582916
  282.2 5.8 %copy-start.7 = (f32[128,1024]{1,0:T(8,128)S(1)}, f32[128,1024]{1,0:T(8,128)}, u32[]{:S(2)}) copy-start(f32[128,1024]{1,0:T(8,128)} %os.1) | copy-start | bytes 1572868
  282.2 5.8 %copy-start.10 = (f32[128,2048]{1,0:T(8,128)S(1)}, f32[128,2048]{1,0:T(8,128)}, u32[]{:S(2)}) copy-start(f32[128,2048]{1,0:T(8,128)} %get-tuple-element.20) | copy-start | bytes 3145732
  285.5 3.0 %copy-start.17 = (bf16[2048,1024]{1,0:T(8,128)(2,1)S(1)}, bf16[2048,1024]{1,0:T(8,128)(2,1)}, u32[]{:S(2)}) copy-start(bf16[2048,1024]{1,0:T(8,128)(2,1)} %get-tuple-element.24) | copy-start | bytes 12582916
  288.3 3.4 %copy-start.8 = (f32[128,1024]{1,0:T(8,128)}, f32[128,1024]{1,0:T(8,128)S(1)}, u32[]{:S(2)}) copy-start(f32[128,1024]{1,0:T(8,128)S(1)} %get-tuple-element.27) | copy-start | bytes 1572868
  288.3 3.4 %copy-start.9 = (f32[128,1024]{1,0:T(8,128)}, f32[128,1024]{1,0:T(8,128)S(1)}, u32[]{:S(2)}) copy-start(f32[128,1024]{1,0:T(8,128)S(1)} %get-tuple-element.28) | copy-start | bytes 1572868
where the time goes:
time: 293 us
  Pallas kernels  271 us (92%)
  matrix products  13.6 us (5%)
  other arithmetic  5.92 us (2%)
    pallas_call x1, Pallas kernels, exchange(): pl.pallas_call(functools.partial(kernel, fs, tp), out_shape=(*(whole(weig...  271 us
    dot_general x6, matrix products, matmul(): return jnp.dot(left, right, preferred_element_type=jnp.float32)  13.6 us

commit v1 on v0

--- a/solution.py
+++ b/solution.py
@@ -39,82 +39,104 @@
 
 
 class Gather:
-    def __init__(self, number, own, whole, me, count, parity, send_sem, recv_sem):
-        self.number, self.own, self.whole, self.me = number, own, whole, me
-        self.count, self.parity = count, parity
+    def __init__(self, number, own, whole, block, half, me, count, by_line, send_sem, recv_sem):
+        self.number, self.whole, self.block, self.half = number, whole, block, half
+        self.me, self.count, self.by_line = me, count, by_line
         self.send_sem, self.recv_sem = send_sem, recv_sem
-        self.rows = whole.shape[0] // count
+        self.rows = block // 2 if half is not None else block
         self.sent = []
         self.relayed = count == 8
-        place, side = me // 2, lax.rem(me, 2)
-        self.cross = place * 2 + (1 - side)
-        self.up = lax.rem(place + 1, 4) * 2 + side
-        self.down = lax.rem(place + 3, 4) * 2 + side
-        up_cross = lax.rem(place + 1, 4) * 2 + (1 - side)
-        down_cross = lax.rem(place + 3, 4) * 2 + (1 - side)
-        far = lax.rem(place + 2, 4) * 2 + side
-        far_cross = lax.rem(place + 2, 4) * 2 + (1 - side)
-        if self.relayed:
-            self.origins = [
-                self.cross, self.down, self.up, down_cross, up_cross, far, far_cross
-            ]
-        else:
-            self.origins = [lax.rem(me + count - k, count) for k in range(1, count)]
+        self.place, self.side = me // 2, lax.rem(me, 2)
+        self.own = self.slot(me) if own is None else own
+
+    def index(self, step, other=False):
+        place = lax.rem(self.place + step + 4, 4)
+        return place * 2 + (1 - self.side if other else self.side)
 
     def slot(self, origin):
-        return self.whole.at[pl.ds(pl.multiple_of(origin * self.rows, self.rows), self.rows), :]
-
-    def copy(self, role, source, origin, target):
-        return pltpu.make_async_remote_copy(
-            src_ref=source,
+        start = pl.multiple_of(origin * self.block, self.block)
+        if self.half:
+            start = pl.multiple_of(start + self.rows, self.rows)
+        return self.whole.at[pl.ds(start, self.rows), :]
+
+    def send(self, role, origin, target, inside=None, source=None):
+        copy = pltpu.make_async_remote_copy(
+            src_ref=self.slot(origin) if source is None else source,
             dst_ref=self.slot(origin),
-            send_sem=self.send_sem.at[self.number, role],
+            send_sem=self.send_sem.at[self.number, len(self.sent)],
             recv_sem=self.recv_sem.at[self.number, role],
             device_id={"fs": target},
             device_id_type=MESH,
         )
-
-    def send(self, role, origin, target, source=None):
-        copy = self.copy(role, self.slot(origin) if source is None else source, origin, target)
-        copy.start()
-        self.sent.append(copy)
-
-    def arrive(self, role):
-        origin = self.origins[role]
-        self.copy(role, self.slot(origin), origin, self.cross).wait_recv()
+        self.sent.append((copy, inside))
+        if inside is None:
+            copy.start()
+        else:
+            pl.when(inside)(copy.start)
+
+    def arrive(self, role, origin, inside=None):
+        copy = pltpu.make_async_remote_copy(
+            src_ref=self.slot(origin),
+            dst_ref=self.slot(origin),
+            send_sem=self.send_sem.at[self.number, 0],
+            recv_sem=self.recv_sem.at[self.number, role],
+            device_id={"fs": lax.rem(self.me + 1, self.count)},
+            device_id_type=MESH,
+        )
+        if inside is None:
+            copy.wait_recv()
+        else:
+            pl.when(inside)(copy.wait_recv)
 
     def start(self):
         if self.relayed:
-            for role, target in enumerate((self.cross, self.up, self.down)):
-                self.send(role, self.me, target, self.own)
+            self.send(0, self.me, self.index(1), self.place < 3, self.own)
+            self.send(3, self.me, self.index(-1), self.place > 0, self.own)
+            self.send(6, self.me, self.index(0, True), None, self.own)
         else:
             for k in range(1, self.count):
-                self.send(k - 1, self.me, lax.rem(self.me + k, self.count), self.own)
-
-    def middle(self):
-        if self.relayed:
-            self.arrive(0)
-            self.send(3, self.origins[0], self.up)
-            self.send(4, self.origins[0], self.down)
-            self.arrive(1)
-            if self.parity:
-                self.send(5, self.origins[1], self.up)
-            self.arrive(2)
-            if not self.parity:
-                self.send(5, self.origins[2], self.down)
-
-    def late(self):
-        if self.relayed:
-            self.arrive(5)
-            self.send(6, self.origins[5], self.cross)
+                self.send(k - 1, self.me, lax.rem(self.me + k, self.count), None, self.own)
+
+    def relay(self, distance):
+        if not self.relayed:
+            return
+        place = self.place
+        across = not (self.by_line and distance == 1)
+        cross = self.index(0, True)
+        if not across:
+            self.arrive(6, cross)
+            self.send(7, cross, self.index(1), place < 3)
+            self.send(10, cross, self.index(-1), place > 0)
+        below, above = self.index(-distance), self.index(distance)
+        from_below, from_above = place >= distance, place + distance < 4
+        self.arrive(distance - 1, below, from_below)
+        if distance < 3:
+            self.send(distance, below, self.index(1), (place >= distance) & (place < 3))
+        if across:
+            self.send(6 + distance, below, cross, from_below)
+        self.arrive(2 + distance, above, from_above)
+        if distance < 3:
+            self.send(3 + distance, above, self.index(-1), from_above & (place > 0))
+        if across:
+            self.send(9 + distance, above, cross, from_above)
 
     def finish(self):
-        for role in (3, 4, 6) if self.relayed else range(self.count - 1):
-            self.arrive(role)
+        if not self.relayed:
+            for k in range(1, self.count):
+                self.arrive(k - 1, lax.rem(self.me + self.count - k, self.count))
+            return
+        if not self.by_line:
+            self.arrive(6, self.index(0, True))
+        for distance in range(1, 4):
+            self.arrive(6 + distance, self.index(-distance, True), self.place >= distance)
+            self.arrive(9 + distance, self.index(distance, True), self.place + distance < 4)
 
     def drain(self):
-        for copy in self.sent:
-            copy.wait_send()
+        for copy, inside in self.sent:
+            if inside is None:
+                copy.wait_send()
+            else:
+                pl.when(inside)(copy.wait_send)
 
 
 def kernel(
@@ -168,13 +190,19 @@
     me, column = lax.axis_index("fs"), lax.axis_index("tp")
     rank, width = qm.shape
     gathers = [
-        Gather(i, own, whole, me, fs, parity, send_sem, recv_sem)
-        for i, (own, whole, parity) in enumerate(
-            ((None, pair_all, 0), (None, ob_all, 1), (qw, qw_all, 0), (vw, vw_all, 1), (ow, ow_all, 0))
-        )
+        Gather(0, None, pair_all, pair_hbm.shape[0], None, me, fs, False, send_sem, recv_sem),
+        Gather(1, None, ob_all, ob_hbm.shape[0], None, me, fs, True, send_sem, recv_sem),
     ]
-    for gather in gathers[:2]:
-        gather.own = gather.slot(me)
+    kept = ((qw, qw_all), (vw, vw_all), (ow, ow_all))
+    for own, whole in kept:
+        block = own.shape[0]
+        for half in range(2):
+            piece = own.at[pl.ds(half * (block // 2), block // 2), :]
+            gathers.append(
+                Gather(
+                    len(gathers), piece, whole, block, half, me, fs, half == 0, send_sem, recv_sem
+                )
+            )
     loads = [
         pltpu.make_async_copy(source, target, local_sem.at[i])
         for i, (source, target) in enumerate(
@@ -206,33 +234,35 @@
         )
     pl.semaphore_wait(barrier, fs + tp - 2)
 
-    pair_g, ob_g, qw_g, vw_g, ow_g = gathers
     loads[0].wait()
-    pair_g.start()
+    gathers[0].start()
     loads[1].wait()
-    ob_g.start()
+    gathers[1].start()
     loads[2].wait()
-    qw_g.start()
-    pair_g.middle()
-    ob_g.middle()
-    pair_g.late()
-    ob_g.late()
+    gathers[2].start()
+    for distance in range(1, 4):
+        gathers[0].relay(distance)
+        gathers[1].relay(distance)
+    gathers[3].start()
     loads[3].wait()
-    vw_g.start()
+    gathers[4].start()
+    gathers[5].start()
     loads[4].wait()
-    ow_g.start()
-    keeps = [
-        pltpu.make_async_copy(gather.own, gather.slot(me), local_sem.at[10 + i])
-        for i, gather in enumerate(gathers[2:])
-    ]
+    gathers[6].start()
+    gathers[7].start()
+    keeps = []
+    for i, (own, whole) in enumerate(kept):
+        rows = own.shape[0]
+        place = whole.at[pl.ds(pl.multiple_of(me * rows, rows), rows), :]
+        keeps.append(pltpu.make_async_copy(own, place, local_sem.at[10 + i]))
     for keep in keeps:
         keep.start()
-    qw_g.middle()
+    gathers[2].relay(1)
     for load in loads[5:]:
         load.wait()
     part[...] = jnp.zeros_like(part)
-    pair_g.finish()
-    ob_g.finish()
+    gathers[0].finish()
+    gathers[1].finish()
 
     tile = 256
 
@@ -271,8 +301,11 @@
         )
         copy.start()
         sums.append(copy)
-    vw_g.middle()
-    qw_g.late()
+    gathers[3].relay(1)
+    gathers[2].relay(2)
+    gathers[4].relay(1)
+    gathers[3].relay(2)
+    gathers[2].relay(3)
 
     def gram(whole, block):
         def add(i, total):
@@ -305,8 +338,13 @@
         )
         copy.start()
         alls.append(copy)
-    ow_g.middle()
-    vw_g.late()
+    gathers[5].relay(1)
+    gathers[4].relay(2)
+    gathers[3].relay(3)
+    gathers[6].relay(1)
+    gathers[5].relay(2)
+    gathers[4].relay(3)
+    gathers[7].relay(1)
     for k in range(1, fs):
         origin = lax.rem(me + fs - k, fs)
         pltpu.make_async_remote_copy(
@@ -335,7 +373,6 @@
         + norm(gram_output, proj[:, 2 * width :], om, os)
     )
     square_own[...] = jnp.broadcast_to(partial, square_own.shape)
-    ow_g.late()
     shares = []
     for k in range(1, tp):
         copy = pltpu.make_async_remote_copy(
@@ -348,6 +385,11 @@
         )
         copy.start()
         shares.append(copy)
+    gathers[6].relay(2)
+    gathers[5].relay(3)
+    gathers[7].relay(2)
+    gathers[6].relay(3)
+    gathers[7].relay(3)
     for copy in shares:
         copy.wait_recv()
     whole_squares = square_own[...]
@@ -369,7 +411,7 @@
     total = sum(grad.shape[1] for grad in grads)
     rank = means[0].shape[0]
     bf16, f32 = jnp.bfloat16, jnp.float32
-    places = max(fs - 1, 7)
+    places = max(fs - 1, 16)
     hbm, vmem = pl.BlockSpec(memory_space=pl.ANY), pl.BlockSpec(memory_space=pltpu.VMEM)
     dma = pltpu.SemaphoreType.DMA
 
@@ -393,8 +435,8 @@
             pltpu.VMEM((fs - 1, share, total), f32),
             pltpu.VMEM((8, 128), f32),
             pltpu.VMEM((tp - 1, 8, 128), f32),
-            dma((5, places)),
-            dma((5, places)),
+            dma((8, places)),
+            dma((8, places)),
             dma((fs - 1,)),
             dma((fs - 1,)),
             dma((fs - 1,)),

time: 293 us -> 216 us (0.74)
  the two profiles are of different devices: /device:TPU:12 before, /device:TPU:0 now
where the time goes in v1:
time: 216 us
  Pallas kernels  193 us (89%)
  matrix products  13.6 us (6%)
  other arithmetic  5.92 us (3%)
    pallas_call x1, Pallas kernels, exchange(): pl.pallas_call(functools.partial(kernel, fs, tp), out_shape=(*(whole(weig...  193 us
    dot_general x6, matrix products, matmul(): return jnp.dot(left, right, preferred_element_type=jnp.float32)  13.6 us

profile of v1, /device:TPU:0, one launch (start us, length us, event | category | flops | bytes accessed | tf_op | source)
XLA Modules:
  0.0 215.8 jit_solution(1822685562017435803)
XLA Ops:
  0.7 1.4 convert_element_type.45.qw_hbm
  2.2 1.3 convert_element_type.46.vw_hbm
  3.4 1.3 convert_element_type.47.ow_hbm
  4.9 193.4 %shard_map.256 = (bf16[4096,512]{1,0:T(8,128)(2,1)}, bf16[4096,512]{1,0:T(8,128)(2,1)}, bf16[2048,1024]{1,0:T(8,128)(2,1)}, bf16[4096,256]{1,0:T(8,128)(2,1)}, b...) custom-call(bf16[1024,4096]{1,0:T(8,128)(2,1)} %mixer_hbm.1, bf16[1024,2048]{1,0:T(8,128)(2,1)} %cell_hbm.1, ...), custom_call_target="tpu_custom_call" | custom-call | tf_op jit(solution)/shard_map/pallas_call | solution.py:421
  198.3 1.4 reduce-precision_convert_fusion.1
  199.7 0.0 copy-start.11
  199.7 0.0 copy-start.12
  199.7 0.0 copy-start.13
  199.7 0.0 copy-start.14
  199.8 0.1 fusion.11
  199.9 0.5 slice.18
  201.4 0.1 fusion.29
  201.5 0.1 copy-done.19
  201.7 3.3 %add_convert_fusion.1 = bf16[4096,512]{1,0:T(8,128)(2,1)} fusion(bf16[4096,512]{1,0:T(8,128)(2,1)S(1)} %copy-done.19, f32[]{:T(128)} %bitcast.1, bf16[4096,128]{1,0:T(8,128)(2,1)S(1)} %get-tuple-element.35, bf16[128,512]{1,0:T(8,128)(2,1)S(1)} %get-tuple-element.41, bf16[128,512]{1,0:T(8,128)(2,1)S(1)} %get-tuple-element.29), kind=kOutput, calls=%fused_computation.1 | convolution fusion | flops 1086849024 | bytes 9699332 | tf_op jit(solution)/shard_map/dot_general | solution.py:23
  204.9 0.0 copy-start.7
  205.0 3.3 %add_convert_fusion.2 = bf16[4096,512]{1,0:T(8,128)(2,1)} fusion(bf16[4096,512]{1,0:T(8,128)(2,1)S(1)} %copy-done.18, f32[]{:T(128)} %bitcast.1, bf16[4096,128]{1,0:T(8,128)(2,1)S(1)} %get-tuple-element.36, bf16[128,512]{1,0:T(8,128)(2,1)S(1)} %get-tuple-element.40, bf16[128,512]{1,0:T(8,128)(2,1)S(1)} %get-tuple-element.37), kind=kOutput, calls=%fused_computation.2 | convolution fusion | flops 1086849024 | bytes 9699332 | tf_op jit(solution)/shard_map/dot_general | solution.py:23
  208.2 1.3 convolution_multiply_fusion.1
  209.5 1.3 convolution_multiply_fusion.2
  210.8 0.3 reduce-precision_convert_fusion
  211.1 0.0 copy-start.8
  211.1 0.0 copy-start.9
  211.1 0.1 fusion.9
  211.2 3.3 %add_convert_fusion = bf16[2048,1024]{1,0:T(8,128)(2,1)} fusion(bf16[2048,1024]{1,0:T(8,128)(2,1)S(1)} %copy-done.17, f32[]{:T(128)} %bitcast.1, bf16[2048,128]{1,0:T(8,128)(2,1)S(1)} %get-tuple-element.25, bf16[128,1024]{1,0:T(8,128)(2,1)S(1)} %fusion.9, bf16[128,1024]{1,0:T(8,128)(2,1)S(1)} %get-tuple-element.26), kind=kOutput, calls=%fused_computation | convolution fusion | flops 1085276160 | bytes 9437188 | tf_op jit(solution)/shard_map/dot_general | solution.py:23
  214.5 1.3 convolution_multiply_fusion
  (33 shorter events, 0.1 us)
Async XLA Ops:
  0.6 4.1 %copy-start.16 = (bf16[512,128]{1,0:T(8,128)(2,1)S(1)}, bf16[512,128]{1,0:T(8,128)(2,1)}, u32[]{:S(2)}) copy-start(bf16[512,128]{1,0:T(8,128)(2,1)} %param.25) | copy-start | bytes 393220
  0.7 4.1 %copy-start.15 = (bf16[512,128]{1,0:T(8,128)(2,1)S(1)}, bf16[512,128]{1,0:T(8,128)(2,1)}, u32[]{:S(2)}) copy-start(bf16[512,128]{1,0:T(8,128)(2,1)} %param.26) | copy-start | bytes 393220
  0.7 4.1 %copy-start.5 = (bf16[256,128]{1,0:T(8,128)(2,1)S(1)}, bf16[256,128]{1,0:T(8,128)(2,1)}, u32[]{:S(2)}) copy-start(bf16[256,128]{1,0:T(8,128)(2,1)} %ob_hbm.1) | copy-start | bytes 196612
  0.7 4.1 %copy-start.1 = (f32[128,512]{1,0:T(8,128)S(1)}, f32[128,512]{1,0:T(8,128)}, u32[]{:S(2)}) copy-start(f32[128,512]{1,0:T(8,128)} %qm.1) | copy-start | bytes 786436
  0.7 4.1 %copy-start.2 = (f32[128,512]{1,0:T(8,128)S(1)}, f32[128,512]{1,0:T(8,128)}, u32[]{:S(2)}) copy-start(f32[128,512]{1,0:T(8,128)} %vm.1) | copy-start | bytes 786436
  0.7 4.1 %copy-start = (f32[128,1024]{1,0:T(8,128)S(1)}, f32[128,1024]{1,0:T(8,128)}, u32[]{:S(2)}) copy-start(f32[128,1024]{1,0:T(8,128)} %om.1) | copy-start | bytes 1572868
  0.7 4.1 %copy-start.3 = (f32[128,512]{1,0:T(8,128)S(1)}, f32[128,512]{1,0:T(8,128)}, u32[]{:S(2)}) copy-start(f32[128,512]{1,0:T(8,128)} %qs.1) | copy-start | bytes 786436
  0.7 4.1 %copy-start.4 = (f32[128,512]{1,0:T(8,128)S(1)}, f32[128,512]{1,0:T(8,128)}, u32[]{:S(2)}) copy-start(f32[128,512]{1,0:T(8,128)} %vs.1) | copy-start | bytes 786436
  198.3 3.1 %copy-start.6 = (bf16[4096,256]{1,0:T(8,128)(2,1)S(1)}, bf16[4096,256]{1,0:T(8,128)(2,1)}, u32[]{:S(2)}) copy-start(bf16[4096,256]{1,0:T(8,128)(2,1)} %get-tuple-element.22) | copy-start | bytes 6291460
  198.3 3.4 %copy-start.19 = (bf16[4096,512]{1,0:T(8,128)(2,1)S(1)}, bf16[4096,512]{1,0:T(8,128)(2,1)}, u32[]{:S(2)}) copy-start(bf16[4096,512]{1,0:T(8,128)(2,1)} %get-tuple-element.23) | copy-start | bytes 12582916
  199.7 5.2 %copy-start.11 = (f32[128,512]{1,0:T(8,128)}, f32[128,512]{1,0:T(8,128)S(1)}, u32[]{:S(2)}) copy-start(f32[128,512]{1,0:T(8,128)S(1)} %get-tuple-element.30) | copy-start | bytes 786436
  199.7 5.2 %copy-start.12 = (f32[128,512]{1,0:T(8,128)}, f32[128,512]{1,0:T(8,128)S(1)}, u32[]{:S(2)}) copy-start(f32[128,512]{1,0:T(8,128)S(1)} %get-tuple-element.31) | copy-start | bytes 786436
  199.7 5.2 %copy-start.13 = (f32[128,512]{1,0:T(8,128)}, f32[128,512]{1,0:T(8,128)S(1)}, u32[]{:S(2)}) copy-start(f32[128,512]{1,0:T(8,128)S(1)} %get-tuple-element.38) | copy-start | bytes 786436
  199.7 5.2 %copy-start.14 = (f32[128,512]{1,0:T(8,128)}, f32[128,512]{1,0:T(8,128)S(1)}, u32[]{:S(2)}) copy-start(f32[128,512]{1,0:T(8,128)S(1)} %get-tuple-element.39) | copy-start | bytes 786436
  201.7 3.3 %copy-start.18 = (bf16[4096,512]{1,0:T(8,128)(2,1)S(1)}, bf16[4096,512]{1,0:T(8,128)(2,1)}, u32[]{:S(2)}) copy-start(bf16[4096,512]{1,0:T(8,128)(2,1)} %get-tuple-element.21) | copy-start | bytes 12582916
  204.9 5.8 %copy-start.7 = (f32[128,1024]{1,0:T(8,128)S(1)}, f32[128,1024]{1,0:T(8,128)}, u32[]{:S(2)}) copy-start(f32[128,1024]{1,0:T(8,128)} %os.1) | copy-start | bytes 1572868
  205.0 5.8 %copy-start.10 = (f32[128,2048]{1,0:T(8,128)S(1)}, f32[128,2048]{1,0:T(8,128)}, u32[]{:S(2)}) copy-start(f32[128,2048]{1,0:T(8,128)} %get-tuple-element.20) | copy-start | bytes 3145732
  208.2 3.0 %copy-start.17 = (bf16[2048,1024]{1,0:T(8,128)(2,1)S(1)}, bf16[2048,1024]{1,0:T(8,128)(2,1)}, u32[]{:S(2)}) copy-start(bf16[2048,1024]{1,0:T(8,128)(2,1)} %get-tuple-element.24) | copy-start | bytes 12582916
  211.1 3.4 %copy-start.8 = (f32[128,1024]{1,0:T(8,128)}, f32[128,1024]{1,0:T(8,128)S(1)}, u32[]{:S(2)}) copy-start(f32[128,1024]{1,0:T(8,128)S(1)} %get-tuple-element.27) | copy-start | bytes 1572868
  211.1 3.4 %copy-start.9 = (f32[128,1024]{1,0:T(8,128)}, f32[128,1024]{1,0:T(8,128)S(1)}, u32[]{:S(2)}) copy-start(f32[128,1024]{1,0:T(8,128)S(1)} %get-tuple-element.28) | copy-start | bytes 1572868

commit v2 on v1

--- a/solution.py
+++ b/solution.py
@@ -181,8 +181,6 @@
     recv_sem,
     sum_send,
     sum_recv,
-    all_send,
-    all_recv,
     tp_send,
     tp_recv,
     local_sem,
@@ -326,35 +324,19 @@
     proj[strip(me), :] = total
     gram_pair = gram(pair_all, 256)
     gram_output = gram(ob_all, 256)
-    alls = []
-    for k in range(1, fs):
-        copy = pltpu.make_async_remote_copy(
-            src_ref=proj.at[strip(me), :],
-            dst_ref=proj.at[strip(me), :],
-            send_sem=all_send.at[k - 1],
-            recv_sem=all_recv.at[k - 1],
-            device_id={"fs": lax.rem(me + k, fs)},
-            device_id_type=MESH,
-        )
-        copy.start()
-        alls.append(copy)
+    strips = Gather(8, None, proj, share, None, me, fs, False, send_sem, recv_sem)
+    strips.start()
     gathers[5].relay(1)
+    strips.relay(1)
     gathers[4].relay(2)
     gathers[3].relay(3)
+    strips.relay(2)
     gathers[6].relay(1)
     gathers[5].relay(2)
+    strips.relay(3)
     gathers[4].relay(3)
     gathers[7].relay(1)
-    for k in range(1, fs):
-        origin = lax.rem(me + fs - k, fs)
-        pltpu.make_async_remote_copy(
-            src_ref=proj.at[strip(origin), :],
-            dst_ref=proj.at[strip(origin), :],
-            send_sem=all_send.at[k - 1],
-            recv_sem=all_recv.at[k - 1],
-            device_id={"fs": lax.rem(me + k, fs)},
-            device_id_type=MESH,
-        ).wait_recv()
+    strips.finish()
 
     def norm(basis_gram, projected, mean, square):
         direction = moments(projected, mean[...], square[...])[2]
@@ -398,9 +380,9 @@
     squares[...] = whole_squares
     for gather in gathers[2:]:
         gather.finish()
-    for copy in sums + alls + shares:
+    for copy in sums + shares:
         copy.wait_send()
-    for gather in gathers:
+    for gather in gathers + [strips]:
         gather.drain()
     for keep in keeps:
         keep.wait()
@@ -435,10 +417,8 @@
             pltpu.VMEM((fs - 1, share, total), f32),
             pltpu.VMEM((8, 128), f32),
             pltpu.VMEM((tp - 1, 8, 128), f32),
-            dma((8, places)),
-            dma((8, places)),
-            dma((fs - 1,)),
-            dma((fs - 1,)),
+            dma((9, places)),
+            dma((9, places)),
             dma((fs - 1,)),
             dma((fs - 1,)),
             dma((tp - 1,)),

time: 216 us -> 216 us (level)
  no operation moved by 1% of the time
where the time goes in v2:
time: 216 us
  Pallas kernels  193 us (89%)
  matrix products  13.6 us (6%)
  other arithmetic  5.92 us (3%)
    pallas_call x1, Pallas kernels, exchange(): pl.pallas_call(functools.partial(kernel, fs, tp), out_shape=(*(whole(weig...  193 us
    dot_general x6, matrix products, matmul(): return jnp.dot(left, right, preferred_element_type=jnp.float32)  13.6 us

profile of v2, /device:TPU:0, one launch (start us, length us, event | category | flops | bytes accessed | tf_op | source)
XLA Modules:
  0.0 215.6 jit_solution(13070214668649573630)
XLA Ops:
  0.7 1.4 convert_element_type.45.qw_hbm
  2.2 1.3 convert_element_type.46.vw_hbm
  3.4 1.3 convert_element_type.47.ow_hbm
  4.9 193.2 %shard_map.256 = (bf16[4096,512]{1,0:T(8,128)(2,1)}, bf16[4096,512]{1,0:T(8,128)(2,1)}, bf16[2048,1024]{1,0:T(8,128)(2,1)}, bf16[4096,256]{1,0:T(8,128)(2,1)}, b...) custom-call(bf16[1024,4096]{1,0:T(8,128)(2,1)} %mixer_hbm.1, bf16[1024,2048]{1,0:T(8,128)(2,1)} %cell_hbm.1, ...), custom_call_target="tpu_custom_call" | custom-call | tf_op jit(solution)/shard_map/pallas_call | solution.py:403
  198.1 1.4 reduce-precision_convert_fusion.1
  199.5 0.0 copy-start.11
  199.5 0.0 copy-start.12
  199.5 0.0 copy-start.13
  199.6 0.0 copy-start.14
  199.6 0.1 fusion.11
  199.7 0.5 slice.18
  201.2 0.1 fusion.29
  201.3 0.1 copy-done.19
  201.5 3.3 %add_convert_fusion.1 = bf16[4096,512]{1,0:T(8,128)(2,1)} fusion(bf16[4096,512]{1,0:T(8,128)(2,1)S(1)} %copy-done.19, f32[]{:T(128)} %bitcast.1, bf16[4096,128]{1,0:T(8,128)(2,1)S(1)} %get-tuple-element.35, bf16[128,512]{1,0:T(8,128)(2,1)S(1)} %get-tuple-element.41, bf16[128,512]{1,0:T(8,128)(2,1)S(1)} %get-tuple-element.29), kind=kOutput, calls=%fused_computation.1 | convolution fusion | flops 1086849024 | bytes 9699332 | tf_op jit(solution)/shard_map/dot_general | solution.py:23
  204.8 0.0 copy-start.7
  204.8 3.3 %add_convert_fusion.2 = bf16[4096,512]{1,0:T(8,128)(2,1)} fusion(bf16[4096,512]{1,0:T(8,128)(2,1)S(1)} %copy-done.18, f32[]{:T(128)} %bitcast.1, bf16[4096,128]{1,0:T(8,128)(2,1)S(1)} %get-tuple-element.36, bf16[128,512]{1,0:T(8,128)(2,1)S(1)} %get-tuple-element.40, bf16[128,512]{1,0:T(8,128)(2,1)S(1)} %get-tuple-element.37), kind=kOutput, calls=%fused_computation.2 | convolution fusion | flops 1086849024 | bytes 9699332 | tf_op jit(solution)/shard_map/dot_general | solution.py:23
  208.1 1.3 convolution_multiply_fusion.1
  209.3 1.3 convolution_multiply_fusion.2
  210.6 0.3 reduce-precision_convert_fusion
  210.9 0.0 copy-start.8
  210.9 0.0 copy-start.9
  210.9 0.1 fusion.9
  211.0 3.3 %add_convert_fusion = bf16[2048,1024]{1,0:T(8,128)(2,1)} fusion(bf16[2048,1024]{1,0:T(8,128)(2,1)S(1)} %copy-done.17, f32[]{:T(128)} %bitcast.1, bf16[2048,128]{1,0:T(8,128)(2,1)S(1)} %get-tuple-element.25, bf16[128,1024]{1,0:T(8,128)(2,1)S(1)} %fusion.9, bf16[128,1024]{1,0:T(8,128)(2,1)S(1)} %get-tuple-element.26), kind=kOutput, calls=%fused_computation | convolution fusion | flops 1085276160 | bytes 9437188 | tf_op jit(solution)/shard_map/dot_general | solution.py:23
  214.3 1.3 convolution_multiply_fusion
  (33 shorter events, 0.1 us)
Async XLA Ops:
  0.6 4.1 %copy-start.16 = (bf16[512,128]{1,0:T(8,128)(2,1)S(1)}, bf16[512,128]{1,0:T(8,128)(2,1)}, u32[]{:S(2)}) copy-start(bf16[512,128]{1,0:T(8,128)(2,1)} %param.25) | copy-start | bytes 393220
  0.7 4.1 %copy-start.15 = (bf16[512,128]{1,0:T(8,128)(2,1)S(1)}, bf16[512,128]{1,0:T(8,128)(2,1)}, u32[]{:S(2)}) copy-start(bf16[512,128]{1,0:T(8,128)(2,1)} %param.26) | copy-start | bytes 393220
  0.7 4.1 %copy-start.5 = (bf16[256,128]{1,0:T(8,128)(2,1)S(1)}, bf16[256,128]{1,0:T(8,128)(2,1)}, u32[]{:S(2)}) copy-start(bf16[256,128]{1,0:T(8,128)(2,1)} %ob_hbm.1) | copy-start | bytes 196612
  0.7 4.1 %copy-start.1 = (f32[128,512]{1,0:T(8,128)S(1)}, f32[128,512]{1,0:T(8,128)}, u32[]{:S(2)}) copy-start(f32[128,512]{1,0:T(8,128)} %qm.1) | copy-start | bytes 786436
  0.7 4.1 %copy-start.2 = (f32[128,512]{1,0:T(8,128)S(1)}, f32[128,512]{1,0:T(8,128)}, u32[]{:S(2)}) copy-start(f32[128,512]{1,0:T(8,128)} %vm.1) | copy-start | bytes 786436
  0.7 4.1 %copy-start = (f32[128,1024]{1,0:T(8,128)S(1)}, f32[128,1024]{1,0:T(8,128)}, u32[]{:S(2)}) copy-start(f32[128,1024]{1,0:T(8,128)} %om.1) | copy-start | bytes 1572868
  0.7 4.1 %copy-start.3 = (f32[128,512]{1,0:T(8,128)S(1)}, f32[128,512]{1,0:T(8,128)}, u32[]{:S(2)}) copy-start(f32[128,512]{1,0:T(8,128)} %qs.1) | copy-start | bytes 786436
  0.7 4.1 %copy-start.4 = (f32[128,512]{1,0:T(8,128)S(1)}, f32[128,512]{1,0:T(8,128)}, u32[]{:S(2)}) copy-start(f32[128,512]{1,0:T(8,128)} %vs.1) | copy-start | bytes 786436
  198.1 3.1 %copy-start.6 = (bf16[4096,256]{1,0:T(8,128)(2,1)S(1)}, bf16[4096,256]{1,0:T(8,128)(2,1)}, u32[]{:S(2)}) copy-start(bf16[4096,256]{1,0:T(8,128)(2,1)} %get-tuple-element.22) | copy-start | bytes 6291460
  198.1 3.4 %copy-start.19 = (bf16[4096,512]{1,0:T(8,128)(2,1)S(1)}, bf16[4096,512]{1,0:T(8,128)(2,1)}, u32[]{:S(2)}) copy-start(bf16[4096,512]{1,0:T(8,128)(2,1)} %get-tuple-element.23) | copy-start | bytes 12582916
  199.5 5.2 %copy-start.11 = (f32[128,512]{1,0:T(8,128)}, f32[128,512]{1,0:T(8,128)S(1)}, u32[]{:S(2)}) copy-start(f32[128,512]{1,0:T(8,128)S(1)} %get-tuple-element.30) | copy-start | bytes 786436
  199.5 5.2 %copy-start.12 = (f32[128,512]{1,0:T(8,128)}, f32[128,512]{1,0:T(8,128)S(1)}, u32[]{:S(2)}) copy-start(f32[128,512]{1,0:T(8,128)S(1)} %get-tuple-element.31) | copy-start | bytes 786436
  199.5 5.2 %copy-start.13 = (f32[128,512]{1,0:T(8,128)}, f32[128,512]{1,0:T(8,128)S(1)}, u32[]{:S(2)}) copy-start(f32[128,512]{1,0:T(8,128)S(1)} %get-tuple-element.38) | copy-start | bytes 786436
  199.6 5.2 %copy-start.14 = (f32[128,512]{1,0:T(8,128)}, f32[128,512]{1,0:T(8,128)S(1)}, u32[]{:S(2)}) copy-start(f32[128,512]{1,0:T(8,128)S(1)} %get-tuple-element.39) | copy-start | bytes 786436
  201.5 3.3 %copy-start.18 = (bf16[4096,512]{1,0:T(8,128)(2,1)S(1)}, bf16[4096,512]{1,0:T(8,128)(2,1)}, u32[]{:S(2)}) copy-start(bf16[4096,512]{1,0:T(8,128)(2,1)} %get-tuple-element.21) | copy-start | bytes 12582916
  204.8 5.8 %copy-start.7 = (f32[128,1024]{1,0:T(8,128)S(1)}, f32[128,1024]{1,0:T(8,128)}, u32[]{:S(2)}) copy-start(f32[128,1024]{1,0:T(8,128)} %os.1) | copy-start | bytes 1572868
  204.8 5.8 %copy-start.10 = (f32[128,2048]{1,0:T(8,128)S(1)}, f32[128,2048]{1,0:T(8,128)}, u32[]{:S(2)}) copy-start(f32[128,2048]{1,0:T(8,128)} %get-tuple-element.20) | copy-start | bytes 3145732
  208.1 3.0 %copy-start.17 = (bf16[2048,1024]{1,0:T(8,128)(2,1)S(1)}, bf16[2048,1024]{1,0:T(8,128)(2,1)}, u32[]{:S(2)}) copy-start(bf16[2048,1024]{1,0:T(8,128)(2,1)} %get-tuple-element.24) | copy-start | bytes 12582916
  210.9 3.4 %copy-start.8 = (f32[128,1024]{1,0:T(8,128)}, f32[128,1024]{1,0:T(8,128)S(1)}, u32[]{:S(2)}) copy-start(f32[128,1024]{1,0:T(8,128)S(1)} %get-tuple-element.27) | copy-start | bytes 1572868
  210.9 3.4 %copy-start.9 = (f32[128,1024]{1,0:T(8,128)}, f32[128,1024]{1,0:T(8,128)S(1)}, u32[]{:S(2)}) copy-start(f32[128,1024]{1,0:T(8,128)S(1)} %get-tuple-element.28) | copy-start | bytes 1572868
